TPU v7x, 32 devices: a whole 2x2x4 slice. The times are simulated.
32 devices in a mesh: dp: 4 (over y, x), kv: 4 (over z), tp: 2 (over core).
Axes of the slice: x: 2, y: 2, z: 4, core: 2. Of those that a mesh axis runs over, the one named last changes fastest.
Arguments:
- tokens: bfloat16 [4096, 2048], P(('dp', 'kv')), parts along dimension 0, may hold values from -7.5 to 7.5
- chosen: int32 [32, 32], P('dp'), parts along dimension 0, may hold values from -1 to 7, as said below
- w_query: bfloat16 [2048, 512], P(None, 'tp'), may hold values from -0.125 to 0.125
- w_key: bfloat16 [2048, 128], P(None, 'tp'), may hold values from -0.125 to 0.125
- w_value: bfloat16 [2048, 128], P(None, 'tp'), may hold values from -0.125 to 0.125
- w_out: bfloat16 [512, 2048], P(None, 'tp'), may hold values from -0.25 to 0.25
- q_gain: float32 [64], replicated, may hold values from 0.1 to 10.5
- k_gain: float32 [64], replicated, may hold values from 0.1 to 10.5
Outputs:
- output: bfloat16 [4096, 2048], P(('dp', 'kv'), 'tp'), parts along dimension 0
There are 4 independent parts, one for each index of `dp`. A program takes and returns all parts, laid end to end along the dimension named above; an argument that names none is the same for every part. Nothing has to cross between parts.
Inputs may be any that keep to these rules, and one draw needn't show every extreme that they name: `chosen`: row b lists the key blocks read by query block b: its live entries come first, are distinct, at most b, and include b; the rest are -1. Over the 2 query blocks of one shard of positions, the live entries name at most one distinct key block of any other shard, and one shard reaches that.
All inputs are finite; a program needn't handle non-finite values.
Results may differ from a plain program's by a relative error of at most 0.0039.
The roundings to bfloat16 on the way count: a program that leaves them out, or rounds other values in their place, can miss the bound.
Values may be sent and summed in bfloat16 or wider, within the bound.
A program may use at most 64 MiB of HBM per device.

v0:
```python
import jax
import jax.numpy as jnp
from jax import lax
from jax.sharding import PartitionSpec as P

HD = 64
BLOCK = 128
NSEL = 32


NEGATIVE = -1e30
EPSILON = 1e-05


def head_norm(values, scale_vec):
    mean_sq = jnp.mean(values * values, axis=-1, keepdims=True)
    return values * lax.rsqrt(mean_sq + EPSILON) * scale_vec


def attend(queries, keyset, valset, block_ids, query_base):
    kv_local = keyset.shape[1]
    group = queries.shape[1] // kv_local
    live_ids = block_ids >= 0
    safe_ids = jnp.maximum(block_ids, 0)
    key_pos = (safe_ids[:, None] * BLOCK + jnp.arange(BLOCK, dtype=jnp.int32)[None, :]).reshape(-1)
    live_keys = jnp.repeat(live_ids, BLOCK)
    query_pos = query_base + jnp.arange(BLOCK, dtype=jnp.int32)
    allowed = live_keys[None, :] & (key_pos[None, :] <= query_pos[:, None])
    grouped = queries.reshape(BLOCK, kv_local, group, HD)
    scores = jnp.einsum(
        "qhgd,khd->hgqk", grouped, keyset, preferred_element_type=jnp.float32
    ) * HD ** (-0.5)
    scores = jnp.where(allowed[None, None], scores, NEGATIVE)
    peak = jnp.max(scores, axis=-1, keepdims=True)
    expd = jnp.exp(scores - peak)
    totals = jnp.sum(expd, axis=-1)
    weights = expd.astype(jnp.bfloat16)
    mixed = jnp.einsum("hgqk,khd->qhgd", weights, valset, preferred_element_type=jnp.float32)
    mixed = mixed / jnp.transpose(totals, (2, 0, 1))[..., None]
    mixed = mixed.reshape(BLOCK, kv_local * group, HD)
    normed = head_norm(mixed, jnp.float32(1.0))
    return normed.astype(jnp.bfloat16).reshape(BLOCK, kv_local * group * HD)


def on_device(tokens, chosen, w_query, w_key, w_value, w_out, q_gain, k_gain):
    row_count = tokens.shape[0]
    q_local = w_query.shape[1] // HD
    kv_local = w_key.shape[1] // HD
    query = head_norm(
        jnp.dot(tokens, w_query, preferred_element_type=jnp.float32).reshape(
            row_count, q_local, HD
        ),
        q_gain,
    ).astype(jnp.bfloat16)
    keyed = head_norm(
        jnp.dot(tokens, w_key, preferred_element_type=jnp.float32).reshape(row_count, kv_local, HD),
        k_gain,
    ).astype(jnp.bfloat16)
    value = jnp.dot(tokens, w_value, preferred_element_type=jnp.float32).astype(jnp.bfloat16)
    packed = jnp.concatenate([keyed.reshape(row_count, kv_local * HD), value], axis=1)
    width = packed.shape[1]
    per_dev = row_count // BLOCK
    my_index = lax.axis_index("kv")
    first_block = my_index * per_dev
    my_lists = lax.dynamic_slice_in_dim(chosen, first_block, per_dev, 0)
    local_blocks = packed.reshape(per_dev, BLOCK, width)
    devices = lax.axis_size("kv")
    asking = chosen.reshape(devices, per_dev * NSEL)
    my_blocks = first_block + jnp.arange(per_dev, dtype=jnp.int32)
    wanted = jnp.any(asking[:, :, None] == my_blocks[None, None, :], axis=1)
    sending = jnp.any(wanted, axis=1) & (jnp.arange(devices, dtype=jnp.int32) != my_index)
    which = jnp.sum(
        wanted.astype(jnp.int32) * jnp.arange(per_dev, dtype=jnp.int32)[None, :], axis=1
    )
    outgoing = jnp.where(sending[:, None, None], local_blocks[which], jnp.zeros((), jnp.bfloat16))
    incoming = lax.all_to_all(outgoing, "kv", split_axis=0, concat_axis=0, tiled=True)
    block_table = jnp.concatenate([incoming, local_blocks], axis=0)
    safe_ids = jnp.maximum(my_lists, 0)
    owners = safe_ids // per_dev
    table_slots = jnp.where(owners == my_index, devices + safe_ids - first_block, owners)
    results = []
    for local_idx in range(per_dev):
        selected = block_table[table_slots[local_idx]]
        keyset = selected[:, :, : kv_local * HD].reshape(NSEL * BLOCK, kv_local, HD)
        valset = selected[:, :, kv_local * HD :].reshape(NSEL * BLOCK, kv_local, HD)
        queries = query[local_idx * BLOCK : (local_idx + 1) * BLOCK]
        results.append(
            attend(queries, keyset, valset, my_lists[local_idx], (first_block + local_idx) * BLOCK)
        )
    attended = jnp.concatenate(results, axis=0)
    summed = jnp.dot(
        lax.all_gather(attended, "tp", axis=1, tiled=True),
        w_out,
        preferred_element_type=jnp.float32,
    )
    return summed.astype(jnp.bfloat16)


def solution(mesh):
    placed = (
        P(("dp", "kv"), None),
        P("dp", None),
        P(None, "tp"),
        P(None, "tp"),
        P(None, "tp"),
        P(None, "tp"),
        P(),
        P(),
    )
    return jax.shard_map(
        on_device, mesh=mesh, in_specs=placed, out_specs=P(("dp", "kv"), "tp"), check_vma=False
    )
```

profile of v0, /device:TPU:0, one launch (start us, length us, event | category | flops | bytes accessed | tf_op | source)
XLA Modules:
  0.0 33.5 jit_solution(11443390478227378669)
XLA Ops:
  0.0 0.0 copy-start
  0.0 0.8 %eq.21 = s32[4,64]{1,0:T(4,128)S(1)} reshape(s32[8,32]{1,0:T(8,128)} %param.9) | data formatting | bytes 2048 | tf_op jit(solution)/shard_map/eq | solution.py:70
  0.9 0.2 compare_reduce_fusion.1
  1.1 1.7 %multiply_reduce_fusion.3 = (f32[256]{0:T(256)S(1)}, f32[256,64]{0,1:T(8,128)S(1)}) fusion(bf16[256,2048]{1,0:T(8,128)(2,1)} %param.8, bf16[2048,64]{0,1:T(8,128)(2,1)} %param.11), kind=kOutput, calls=%fused_computation.40 | convolution fusion | flops 67141376 | bytes 1377280 | tf_op jit(solution)/shard_map/dot_general | solution.py:56
  2.9 0.7 %multiply_convert_fusion.1 = bf16[256,64]{0,1:T(8,128)(2,1)S(1)} fusion(f32[256,64]{0,1:T(8,128)S(1)} %get-tuple-element.20, f32[64]{0:T(128)} %param.15, f32[256]{0:T(256)S(1)} %add_rsqrt_fusion.3), kind=kLoop, calls=%fused_computation.39 | loop fusion | flops 49152 | bytes 99584 | tf_op jit(solution)/shard_map/convert_element_type | solution.py:58
  3.6 0.1 copy.29
  3.7 1.7 %convolution_convert_fusion.1 = bf16[256,64]{0,1:T(8,128)(2,1)S(1)} fusion(bf16[256,2048]{1,0:T(8,128)(2,1)} %param.8, bf16[2048,64]{0,1:T(8,128)(2,1)} %param.12), kind=kOutput, calls=%fused_computation.24 | convolution fusion | flops 67125248 | bytes 1343488 | tf_op jit(solution)/shard_map/dot_general | solution.py:59
  5.4 0.1 copy.30
  5.6 0.1 pad_maximum_fusion.1
  5.7 0.6 %gather_fusion = bf16[4,128,128]{2,1,0:T(8,128)(2,1)S(1)} fusion(bf16[2,128,128]{2,1,0:T(8,128)(2,1)S(1)} %pad_maximum_fusion.1, s32[1024]{0:T(1024)S(1)} %pad_clamp_fusion.2), kind=kCustom, calls=%fused_computation | custom fusion | bytes 262160 | tf_op jit(solution)/shard_map/gather | solution.py:75
  6.2 0.7 %broadcast_select_fusion = bf16[4,128,128]{2,1,0:T(8,128)(2,1)} fusion(bf16[4,128,128]{2,1,0:T(8,128)(2,1)S(1)} %gather_fusion, pred[4]{0:T(512)(128)(4,1)S(1)} %compare_and_fusion.2), kind=kLoop, calls=%fused_computation.35 | loop fusion | flops 65536 | bytes 262148 | tf_op jit(solution)/shard_map/jit(_where)/select_n | solution.py:75
  7.0 6.4 %all-to-all-start = ((bf16[4,128,128]{2,1,0:T(8,128)(2,1)}), bf16[4,128,128]{2,1,0:T(8,128)(2,1)S(1)}, u32[]{:S(2)}, u32[]{:S(2)}) async-start(bf16[4,128,128]{2,1,0:T(8,128)(2,1)} %broadcast_select_fusion), calls=%async_computation | async-start | bytes 262144 | tf_op jit(solution)/shard_map/all_to_all | solution.py:76
  13.3 0.7 %compare_select_fusion = (s32[2,32]{1,0:T(2,128)S(1)}, s32[2,32]{1,0:T(2,128)S(1)}) fusion(s32[]{:T(128)S(6)} %mul.128, s32[]{:T(128)S(6)} %axis_index.15, s32[8,32]{1,0:T(8,128)} %param.9, s32[]{:T(128)S(6)} %select_n.54), kind=kLoop, calls=%fused_computation.51 | loop fusion | flops 832 | bytes 780 | tf_op jit(solution)/shard_map/jit(_where)/select_n | solution.py:80
  14.1 2.1 %multiply_reduce_fusion = (f32[256,4]{0,1:T(4,128)S(1)}, f32[256,256]{0,1:T(8,128)S(1)}) fusion(bf16[256,2048]{1,0:T(8,128)(2,1)} %param.8, bf16[2048,256]{1,0:T(8,128)(2,1)} %param.10), kind=kOutput, calls=%fused_computation.26 | convolution fusion | flops 268565504 | bytes 2363392 | tf_op jit(solution)/shard_map/dot_general | solution.py:50
  16.2 0.1 add_bitcast_fusion
  16.3 0.1 broadcast_bitcast_fusion
  16.4 1.4 %compare_and_fusion.1 = pred[128,4096]{0,1:T(8,128)(4,1)S(1)} fusion(s32[128]{0:T(128)S(1)} %iota_add_fusion.1, s32[4096]{0:T(1024)S(1)} %get-tuple-element.34, pred[4096]{0:T(1024)(128)(4,1)S(1)} %get-tuple-element.36), kind=kLoop, calls=%fused_computation.18 | loop fusion | flops 1048576 | bytes 545280 | tf_op jit(solution)/shard_map/and | solution.py:28
  17.8 1.4 %compare_and_fusion = pred[128,4096]{0,1:T(8,128)(4,1)S(1)} fusion(s32[128]{0:T(128)S(1)} %iota_add_fusion, s32[4096]{0:T(1024)S(1)} %get-tuple-element.33, pred[4096]{0:T(1024)(128)(4,1)S(1)} %get-tuple-element.35), kind=kLoop, calls=%fused_computation.17 | loop fusion | flops 1048576 | bytes 545280 | tf_op jit(solution)/shard_map/and | solution.py:28
  19.2 0.7 %multiply_convert_fusion = bf16[256,4,64]{0,2,1:T(8,128)(2,1)S(1)} fusion(f32[64]{0:T(128)} %param.14, f32[256,4]{0,1:T(4,128)S(1)} %add_rsqrt_fusion, f32[256,256]{0,1:T(8,128)S(1)} %get-tuple-element.22), kind=kLoop, calls=%fused_computation.25 | loop fusion | flops 196608 | bytes 397568 | tf_op jit(solution)/shard_map/convert_element_type | solution.py:54
  19.9 0.0 copy-start.1
  19.9 0.0 all-to-all-done
  19.9 0.1 maximum_maximum_fusion
  20.0 0.7 %gather_fusion.1 = bf16[32,128,128]{2,1,0:T(8,128)(2,1)S(1)} fusion(bf16[6,128,128]{2,1,0:T(8,128)(2,1)S(1)} %maximum_maximum_fusion, s32[1024]{0:T(1024)S(1)} %get-tuple-element.32), kind=kCustom, calls=%fused_computation.1 | custom fusion | bytes 2097280 | tf_op jit(solution)/shard_map/gather | solution.py:83
  20.8 0.5 %fusion.31 = (bf16[32,128,64]{2,1,0:T(8,128)(2,1)S(1)}, bf16[32,128,64]{2,1,0:T(8,128)(2,1)S(1)}) fusion(bf16[32,128,128]{2,1,0:T(8,128)(2,1)S(1)} %gather_fusion.1), kind=kLoop, calls=%fused_computation.72 | loop fusion | bytes 2097152 | tf_op jit(solution)/shard_map/slice | solution.py:84
  21.3 1.2 %fusion.34 = (f32[4,128]{1,0:T(4,128)S(1)}, f32[1,4,128,4096]{2,3,1,0:T(8,128)S(1)}) fusion(bf16[4096,64,1]{1,0,2:T(8,128)(2,1)S(1)} %bitcast.124, bf16[256,4,64]{0,2,1:T(8,128)(2,1)S(1)} %multiply_convert_fusion, pred[128,4096]{0,1:T(8,128)(4,1)S(1)} %compare_and_fusion.1), kind=kOutput, calls=%fused_computation.75 | convolution fusion | flops 274726400 | bytes 10029056 | tf_op jit(solution)/shard_map/qhgd,khd->hgqk/dot_general | solution.py:30
  22.5 0.0 copy-done.1
  22.5 1.1 %fusion = f32[4,128]{1,0:T(4,128)S(1)} fusion(f32[1,4,128,4096]{2,3,1,0:T(8,128)S(1)} %get-tuple-element.28, f32[4,128]{1,0:T(4,128)S(1)} %get-tuple-element.27), kind=kLoop, calls=%fused_computation.7 | loop fusion | flops 4193792 | bytes 8392704 | tf_op jit(solution)/shard_map/reduce_sum | solution.py:36
  23.6 0.0 copy-start.2
  23.6 1.4 %multiply_reduce_fusion.2 = (f32[128,4]{0,1:T(4,128)S(1)}, f32[128,1,4,64]{0,3,2,1:T(8,128)S(1)}) fusion(f32[128,4]{0,1:T(4,128)S(1)} %bitcast.129, bf16[4096,64,1]{1,0,2:T(8,128)(2,1)S(1)} %bitcast.122, f32[1,4,128,4096]{2,3,1,0:T(8,128)S(1)} %get-tuple-element.28, f32[4,128]{1,0:T(4,128)S(1)} %get-tuple-element.27), kind=kOutput, calls=%fused_computation.34 | convolution fusion | flops 272727552 | bytes 9050112 | tf_op jit(solution)/shard_map/hgqk,khd->qhgd/dot_general | solution.py:38
  25.1 0.8 %gather_fusion.2 = bf16[32,128,128]{2,1,0:T(8,128)(2,1)S(1)} fusion(bf16[6,128,128]{2,1,0:T(8,128)(2,1)S(1)} %maximum_maximum_fusion, s32[1024]{0:T(1024)S(1)} %get-tuple-element.31), kind=kCustom, calls=%fused_computation.2 | custom fusion | bytes 2097280 | tf_op jit(solution)/shard_map/gather | solution.py:83
  25.8 0.5 %fusion.32 = (bf16[32,128,64]{2,1,0:T(8,128)(2,1)S(1)}, bf16[32,128,64]{2,1,0:T(8,128)(2,1)S(1)}) fusion(bf16[32,128,128]{2,1,0:T(8,128)(2,1)S(1)} %gather_fusion.2), kind=kLoop, calls=%fused_computation.73 | loop fusion | bytes 2097152 | tf_op jit(solution)/shard_map/slice | solution.py:84
  26.3 0.0 copy-done.2
  26.3 1.2 %fusion.33 = (f32[4,128]{1,0:T(4,128)S(1)}, f32[1,4,128,4096]{2,3,1,0:T(8,128)S(1)}) fusion(bf16[4096,64,1]{1,0,2:T(8,128)(2,1)S(1)} %bitcast.123, bf16[256,4,64]{0,2,1:T(8,128)(2,1)S(1)} %copy-done.2, pred[128,4096]{0,1:T(8,128)(4,1)S(1)} %compare_and_fusion), kind=kOutput, calls=%fused_computation.74 | convolution fusion | flops 274726400 | bytes 10029056 | tf_op jit(solution)/shard_map/qhgd,khd->hgqk/dot_general | solution.py:30
  27.6 1.1 %fusion.2 = f32[4,128]{1,0:T(4,128)S(1)} fusion(f32[1,4,128,4096]{2,3,1,0:T(8,128)S(1)} %get-tuple-element.24, f32[4,128]{1,0:T(4,128)S(1)} %get-tuple-element.23), kind=kLoop, calls=%fused_computation.9 | loop fusion | flops 4193792 | bytes 8392704 | tf_op jit(solution)/shard_map/reduce_sum | solution.py:36
  28.7 1.4 %multiply_reduce_fusion.1 = (f32[128,4]{0,1:T(4,128)S(1)}, f32[128,1,4,64]{0,3,2,1:T(8,128)S(1)}) fusion(f32[128,4]{0,1:T(4,128)S(1)} %bitcast.130, bf16[4096,64,1]{1,0,2:T(8,128)(2,1)S(1)} %bitcast.121, f32[1,4,128,4096]{2,3,1,0:T(8,128)S(1)} %get-tuple-element.24, f32[4,128]{1,0:T(4,128)S(1)} %get-tuple-element.23), kind=kOutput, calls=%fused_computation.33 | convolution fusion | flops 272727552 | bytes 9050112 | tf_op jit(solution)/shard_map/hgqk,khd->qhgd/dot_general | solution.py:38
  30.2 2.0 %all_gather.3 = bf16[256,512]{0,1:T(8,128)(2,1)S(1)} all-gather(bf16[256,256]{0,1:T(8,128)(2,1)S(1)} %pad_maximum_fusion), channel_id=1, replica_groups=mesh['dp'=4,'kv'=4,'tp'=2] {'tp'}, dimensions={1}, use_global_device_ids=true | all-gather | bytes 393216 | tf_op jit(solution)/shard_map/all_gather | solution.py:92
  32.2 0.0 copy-done
  32.2 1.3 %convolution_convert_fusion = bf16[256,1024]{1,0:T(8,128)(2,1)} fusion(bf16[256,512]{0,1:T(8,128)(2,1)S(1)} %all_gather.3, bf16[512,1024]{1,0:T(8,128)(2,1)S(1)} %copy-done), kind=kOutput, calls=%fused_computation.19 | convolution fusion | flops 268697600 | bytes 1835008 | tf_op jit(solution)/shard_map/dot_general | solution.py:91
  (18 shorter events, 0.2 us)
Async XLA Ops:
  0.0 32.2 %copy-start = (bf16[512,1024]{1,0:T(8,128)(2,1)S(1)}, bf16[512,1024]{1,0:T(8,128)(2,1)}, u32[]{:S(2)}) copy-start(bf16[512,1024]{1,0:T(8,128)(2,1)} %param.13) | copy-start | bytes 3145732
  7.0 12.9 %all-to-all-start = ((bf16[4,128,128]{2,1,0:T(8,128)(2,1)}), bf16[4,128,128]{2,1,0:T(8,128)(2,1)S(1)}, u32[]{:S(2)}, u32[]{:S(2)}) async-start(bf16[4,128,128]{2,1,0:T(8,128)(2,1)} %broadcast_select_fusion), calls=%async_computation | async-start | bytes 262144 | tf_op jit(solution)/shard_map/all_to_all | solution.py:76
  19.9 2.6 %copy-start.1 = (bf16[256,4,64]{0,2,1:T(8,128)(2,1)}, bf16[256,4,64]{0,2,1:T(8,128)(2,1)S(1)}, u32[]{:S(2)}) copy-start(bf16[256,4,64]{0,2,1:T(8,128)(2,1)S(1)} %multiply_convert_fusion) | copy-start | bytes 393220
  23.6 2.7 %copy-start.2 = (bf16[256,4,64]{0,2,1:T(8,128)(2,1)S(1)}, bf16[256,4,64]{0,2,1:T(8,128)(2,1)}, u32[]{:S(2)}) copy-start(bf16[256,4,64]{0,2,1:T(8,128)(2,1)} %copy-done.1) | copy-start | bytes 393220
where the time goes:
time: 33.8 us; the launch traced here: 33.5 us
  matrix products  12.1 us (36%)
  other arithmetic  8.57 us (25%)
  starting transfers between devices  6.35 us (19%)
  local copies, waits for them, and re-layouts  4.16 us (12%)
  blocking collectives  1.99 us (6%)
    all_to_all x1, starting transfers between devices, on_device(): lax.all_to_all(outgoing, 'kv', split_axis=0, concat_axis=0, tiled=True)  6.35 us
    dot_general x2, matrix products, attend(): jnp.einsum('hgqk,khd->qhgd', weights, valset, preferred_element_type=jnp....  2.86 us
    and x2, other arithmetic, attend(): allowed = live_keys[None, :] & (key_pos[None, :] <= query_pos[:, None])  2.78 us
    dot_general x2, matrix products, attend(): jnp.einsum('qhgd,khd->hgqk', grouped, keyset, preferred_element_type=jnp....  2.49 us
    reduce_sum x2, other arithmetic, attend(): totals = jnp.sum(expd, axis=-1)  2.24 us
    dot_general x1, matrix products, on_device(): jnp.dot(tokens, w_query, preferred_element_type=jnp.float32)  2.08 us
    all_gather x1, blocking collectives, on_device(): lax.all_gather(attended, 'tp', axis=1, tiled=True)  1.99 us
    dot_general x1, matrix products, on_device(): jnp.dot(tokens, w_key, preferred_element_type=jnp.float32)  1.72 us
  transfers between devices with their start and end apart: 1, of which 0 were waited for; matrix products, arithmetic and copies ran while one was open for 19% of the time, Pallas kernels for 0%

commit v1 on v0

v1 whole, which is shorter than its diff:
```python
import functools

import jax
import jax.numpy as jnp
from jax import lax
from jax.experimental import pallas as pl
from jax.experimental.pallas import tpu as pltpu
from jax.sharding import PartitionSpec as P

HD = 64
BLOCK = 128
NEGATIVE = -1e30
EPSILON = 1e-05
MESH = pl.DeviceIdType.MESH
F32 = jnp.float32
BF16 = jnp.bfloat16


def repeat(count, body):
    if count <= 8:
        for i in range(count):
            body(i)
    else:
        lax.fori_loop(0, count, lambda i, c: (body(i), c)[1], 0)


def dot_nt(a, b):
    return lax.dot_general(a, b, (((1,), (1,)), ((), ())), preferred_element_type=F32)


def kernel(
    kv_n, tp_n, group,
    chosen_ref, qg_ref, kg_ref, tok_hbm, wq_hbm, wk_hbm, wv_hbm, wo_hbm,
    out_ref,
    tok, wq, wkv, wo, local, stage, slots, queries, mine, theirs,
    load_sem, kv_send, kv_recv, tp_send, tp_recv,
):
    me = lax.axis_index("kv")
    core = lax.axis_index("tp")
    rows = tok.shape[0]
    per_dev = rows // BLOCK
    q_width = wq.shape[1]
    heads = q_width // HD
    first = me * per_dev

    loads = [
        pltpu.make_async_copy(wk_hbm, wkv.at[pl.ds(0, HD)], load_sem.at[0]),
        pltpu.make_async_copy(wv_hbm, wkv.at[pl.ds(HD, HD)], load_sem.at[1]),
        pltpu.make_async_copy(tok_hbm, tok, load_sem.at[2]),
        pltpu.make_async_copy(wq_hbm, wq, load_sem.at[3]),
        pltpu.make_async_copy(wo_hbm, wo, load_sem.at[4]),
    ]
    for load in loads:
        load.start()

    barrier = pltpu.get_barrier_semaphore()

    def greet(i):
        pl.semaphore_signal(
            barrier, inc=1, device_id={"kv": lax.rem(me + i + 1, kv_n)}, device_id_type=MESH
        )

    repeat(kv_n - 1, greet)
    for r in range(1, tp_n):
        pl.semaphore_signal(
            barrier, inc=1, device_id={"tp": lax.rem(core + r, tp_n)}, device_id_type=MESH
        )

    chosen = chosen_ref[...]
    row_id = lax.broadcasted_iota(jnp.int32, chosen.shape, 0)

    def found(cond):
        return jnp.max(jnp.where(cond, 1.0, 0.0), axis=(0, 1), keepdims=True)

    for load in loads[:3]:
        load.wait()
    kv = dot_nt(tok[...], wkv[...])
    lane = lax.broadcasted_iota(jnp.int32, (rows, 2 * HD), 1)
    is_key = lane < HD
    mean_sq = jnp.sum(jnp.where(is_key, kv * kv, 0.0), axis=-1, keepdims=True) * (1.0 / HD)
    gain = jnp.concatenate([kg_ref[...], jnp.ones((1, HD), F32)], axis=1)
    packed = jnp.where(is_key, kv * lax.rsqrt(mean_sq + EPSILON), kv) * gain
    local[...] = packed.astype(BF16)

    def fill(i):
        dest = me + i + 1

        @pl.when(dest < kv_n)
        def _():
            asked = (row_id >= dest * per_dev) & (row_id < (dest + 1) * per_dev)
            sel = packed[:BLOCK]
            for j in range(1, per_dev):
                hit = jnp.broadcast_to(found(asked & (chosen == first + j)), sel.shape)
                sel = jnp.where(hit > 0.5, packed[j * BLOCK : (j + 1) * BLOCK], sel)
            stage[i] = sel.astype(BF16)

        @pl.when(me - i - 1 < 0)
        def _():
            slots[i] = jnp.zeros(slots.shape[1:], BF16)

    repeat(kv_n - 1, fill)

    pl.semaphore_wait(barrier, kv_n - 1 + tp_n - 1)

    def kv_copy(i):
        return pltpu.make_async_remote_copy(
            src_ref=stage.at[i],
            dst_ref=slots.at[i],
            send_sem=kv_send.at[i],
            recv_sem=kv_recv.at[i],
            device_id={"kv": lax.rem(me + i + 1, kv_n)},
            device_id_type=MESH,
        )

    def send(i):
        far = kv_n - 2 - i

        @pl.when(me + far + 1 < kv_n)
        def _():
            kv_copy(far).start()

    repeat(kv_n - 1, send)

    loads[3].wait()
    query = jnp.dot(tok[...], wq[...], preferred_element_type=F32)
    for h in range(heads):
        qh = query[:, h * HD : (h + 1) * HD]
        q_sq = jnp.mean(qh * qh, axis=-1, keepdims=True)
        qh = (qh * lax.rsqrt(q_sq + EPSILON) * qg_ref[...] * HD**-0.5).astype(BF16)
        qh = jnp.concatenate([qh, jnp.zeros((rows, HD), BF16)], axis=1)
        for lb in range(per_dev):
            queries[lb, h * BLOCK : (h + 1) * BLOCK] = qh[lb * BLOCK : (lb + 1) * BLOCK]

    lane_row = lax.broadcasted_iota(jnp.int32, (1, 2 * HD), 1)
    keep = jnp.where(lane_row < HD, 0.0, 1.0).astype(BF16)
    ones = jnp.where(lane_row < HD, 1.0, 0.0).astype(BF16)

    def with_ones(block):
        return block * keep + ones

    q_pos = lax.rem(
        lax.broadcasted_iota(jnp.int32, (heads * BLOCK, BLOCK), 0), BLOCK
    )
    causal = lax.broadcasted_iota(jnp.int32, (heads * BLOCK, BLOCK), 1) <= q_pos

    def bias_of(cond):
        return jnp.broadcast_to((1.0 - found(cond)) * NEGATIVE, (1, BLOCK))

    state = []
    for lb in range(per_dev):
        mine_row = row_id == first + lb
        scores = dot_nt(queries[lb], local[: (lb + 1) * BLOCK])
        parts = [
            scores[:, j * BLOCK : (j + 1) * BLOCK] + bias_of(mine_row & (chosen == first + j))
            for j in range(lb)
        ]
        parts.append(jnp.where(causal, scores[:, lb * BLOCK :], NEGATIVE))
        scores = jnp.concatenate(parts, axis=1) if lb else parts[0]
        peak = jnp.max(scores, axis=-1, keepdims=True)
        weights = jnp.exp(scores - peak).astype(BF16)
        acc = jnp.dot(
            weights, with_ones(local[: (lb + 1) * BLOCK]), preferred_element_type=F32
        )
        state.append((peak, acc))

    def arrive(i):
        @pl.when(me - i - 1 >= 0)
        def _():
            kv_copy(i).wait_recv()

    def merge(lb, base, peak, acc):
        mine_row = row_id == first + lb
        keyset = slots[pl.ds(base, group)].reshape(group * BLOCK, 2 * HD)
        biases = []
        for g in range(group):
            low = (me - base - g - 1) * per_dev
            biases.append(
                bias_of(mine_row & (chosen >= 0) & (chosen >= low) & (chosen < low + per_dev))
            )
        scores = dot_nt(queries[lb], keyset) + jnp.concatenate(biases, axis=1)
        peak_now = jnp.maximum(peak, jnp.max(scores, axis=-1, keepdims=True))
        weights = jnp.exp(scores - peak_now).astype(BF16)
        acc = acc * jnp.exp(peak - peak_now) + jnp.dot(
            weights, with_ones(keyset), preferred_element_type=F32
        )
        return peak_now, acc

    def tp_copy(r, lb):
        return pltpu.make_async_remote_copy(
            src_ref=mine.at[lb],
            dst_ref=theirs.at[r - 1, lb],
            send_sem=tp_send.at[r - 1, lb],
            recv_sem=tp_recv.at[r - 1, lb],
            device_id={"tp": lax.rem(core + r, tp_n)},
            device_id_type=MESH,
        )

    repeat(kv_n - 1, arrive)
    groups = (kv_n - 1) // group
    for lb in range(per_dev):
        peak, acc = state[lb]
        if groups <= 2:
            for n in range(groups):
                peak, acc = merge(lb, n * group, peak, acc)
        else:
            peak, acc = lax.fori_loop(
                0, groups, lambda n, c: merge(lb, n * group, *c), (peak, acc)
            )
        totals = acc[:, :1]
        mixed = acc[:, HD:]
        m_sq = jnp.mean(mixed * mixed, axis=-1, keepdims=True)
        normed = mixed * lax.rsqrt(m_sq + EPSILON * totals * totals)
        for h in range(heads):
            mine[lb, :, h * HD : (h + 1) * HD] = normed[h * BLOCK : (h + 1) * BLOCK].astype(BF16)
        for r in range(1, tp_n):
            tp_copy(r, lb).start()

    loads[4].wait()
    own_w = wo[pl.ds(pl.multiple_of(core * q_width, q_width), q_width), :]
    for lb in range(per_dev):
        total = jnp.dot(mine[lb], own_w, preferred_element_type=F32)
        for r in range(1, tp_n):
            tp_copy(r, lb).wait_recv()
            src = lax.rem(core - r + tp_n, tp_n)
            src_w = wo[pl.ds(pl.multiple_of(src * q_width, q_width), q_width), :]
            total = total + jnp.dot(theirs[r - 1, lb], src_w, preferred_element_type=F32)
        out_ref[lb * BLOCK : (lb + 1) * BLOCK, :] = total.astype(BF16)

    def sent(i):
        @pl.when(me + i + 1 < kv_n)
        def _():
            kv_copy(i).wait_send()

    repeat(kv_n - 1, sent)
    for lb in range(per_dev):
        for r in range(1, tp_n):
            tp_copy(r, lb).wait_send()


def on_device(kv_n, tp_n, tokens, chosen, w_query, w_key, w_value, w_out, q_gain, k_gain):
    rows, depth = tokens.shape
    q_width = w_query.shape[1]
    per_dev = rows // BLOCK
    heads = q_width // HD
    group = next(g for g in (3, 2, 1) if (kv_n - 1) % g == 0)
    vmem = pl.BlockSpec(memory_space=pltpu.VMEM)
    hbm = pl.BlockSpec(memory_space=pl.ANY)
    return pl.pallas_call(
        functools.partial(kernel, kv_n, tp_n, group),
        out_shape=jax.ShapeDtypeStruct((rows, w_out.shape[1]), BF16),
        in_specs=[vmem] * 3 + [hbm] * 5,
        out_specs=vmem,
        scratch_shapes=[
            pltpu.VMEM((rows, depth), BF16),
            pltpu.VMEM((depth, q_width), BF16),
            pltpu.VMEM((2 * HD, depth), BF16),
            pltpu.VMEM(w_out.shape, BF16),
            pltpu.VMEM((rows, 2 * HD), BF16),
            pltpu.VMEM((kv_n - 1, BLOCK, 2 * HD), BF16),
            pltpu.VMEM((kv_n - 1, BLOCK, 2 * HD), BF16),
            pltpu.VMEM((per_dev, heads * BLOCK, 2 * HD), BF16),
            pltpu.VMEM((per_dev, BLOCK, q_width), BF16),
            pltpu.VMEM((tp_n - 1, per_dev, BLOCK, q_width), BF16),
            pltpu.SemaphoreType.DMA((5,)),
            pltpu.SemaphoreType.DMA((kv_n - 1,)),
            pltpu.SemaphoreType.DMA((kv_n - 1,)),
            pltpu.SemaphoreType.DMA((tp_n - 1, per_dev)),
            pltpu.SemaphoreType.DMA((tp_n - 1, per_dev)),
        ],
        compiler_params=pltpu.CompilerParams(collective_id=0, has_side_effects=True),
    )(
        chosen, q_gain.reshape(1, HD), k_gain.reshape(1, HD),
        tokens, w_query, w_key.T, w_value.T, w_out,
    )


def solution(mesh):
    placed = (
        P(("dp", "kv"), None),
        P("dp", None),
        P(None, "tp"),
        P(None, "tp"),
        P(None, "tp"),
        P(None, "tp"),
        P(),
        P(),
    )
    return jax.shard_map(
        functools.partial(on_device, mesh.shape["kv"], mesh.shape["tp"]),
        mesh=mesh, in_specs=placed, out_specs=P(("dp", "kv"), "tp"), check_vma=False,
    )
```

time: 33.8 us -> 14.3 us (0.42)
  the two profiles are of different devices: /device:TPU:0 before, /device:TPU:9 now
where the time goes in v1:
time: 14.3 us; the launch traced here: 14.1 us
  Pallas kernels  12.2 us (85%)
  local copies, waits for them, and re-layouts  1.87 us (13%)
    pallas_call x1, Pallas kernels, on_device(): pl.pallas_call(functools.partial(kernel, kv_n, tp_n, group), out_shape=ja...  12.2 us
    unnamed x1, local copies, waits for them, and re-layouts  1.87 us

profile of v1, /device:TPU:9, one launch (start us, length us, event | category | flops | bytes accessed | tf_op | source)
XLA Modules:
  0.0 14.1 jit_solution(16770515186424731944)
XLA Ops:
  0.0 12.2 %shard_map.82 = bf16[256,1024]{1,0:T(8,128)(2,1)} custom-call(s32[8,32]{1,0:T(8,128)} %chosen_ref.1, f32[1,64]{1,0:T(1,128)} %bitcast.6, f32[1,64]{1,0:T(1,128)} %bitcast.7, bf16[256,2048]{1,0:T(8,128)(2,1)} %tok_hbm.1, bf16[2048,256]{1,0:T(8,128)(2,1)} %wq_hbm.1, bf16[64,2048]{1,0:T(8,128)(2,1)} %bitcast.4, bf16[64,2048]{1,0:T(8,128)(2,1)} %bitcast.5, ...), custom_call_target="tpu_custom_call" | custom-call | tf_op jit(solution)/shard_map/pallas_call | solution.py:248
  12.3 1.9 %copy.10 = bf16[256,1024]{1,0:T(8,128)(2,1)} copy(bf16[256,1024]{1,0:T(8,128)(2,1)} %shard_map.82) | data formatting | bytes 1048576

commit v2 on v1

--- a/solution.py
+++ b/solution.py
@@ -30,9 +30,9 @@
 
 def kernel(
     kv_n, tp_n, group,
-    chosen_ref, qg_ref, kg_ref, tok_hbm, wq_hbm, wk_hbm, wv_hbm, wo_hbm,
+    chosen_hbm, qg_hbm, kg_hbm, tok_hbm, wq_hbm, wk_hbm, wv_hbm,
     out_ref,
-    tok, wq, wkv, wo, local, stage, slots, queries, mine, theirs,
+    chosen_ref, qg_ref, kg_ref, tok, wq, wkv, local, stage, slots, queries, mine, theirs,
     load_sem, kv_send, kv_recv, tp_send, tp_recv,
 ):
     me = lax.axis_index("kv")
@@ -47,8 +47,10 @@
         pltpu.make_async_copy(wk_hbm, wkv.at[pl.ds(0, HD)], load_sem.at[0]),
         pltpu.make_async_copy(wv_hbm, wkv.at[pl.ds(HD, HD)], load_sem.at[1]),
         pltpu.make_async_copy(tok_hbm, tok, load_sem.at[2]),
-        pltpu.make_async_copy(wq_hbm, wq, load_sem.at[3]),
-        pltpu.make_async_copy(wo_hbm, wo, load_sem.at[4]),
+        pltpu.make_async_copy(chosen_hbm, chosen_ref, load_sem.at[3]),
+        pltpu.make_async_copy(qg_hbm, qg_ref, load_sem.at[4]),
+        pltpu.make_async_copy(kg_hbm, kg_ref, load_sem.at[5]),
+        pltpu.make_async_copy(wq_hbm, wq, load_sem.at[6]),
     ]
     for load in loads:
         load.start()
@@ -66,14 +68,16 @@
             barrier, inc=1, device_id={"tp": lax.rem(core + r, tp_n)}, device_id_type=MESH
         )
 
-    chosen = chosen_ref[...]
-    row_id = lax.broadcasted_iota(jnp.int32, chosen.shape, 0)
-
     def found(cond):
         return jnp.max(jnp.where(cond, 1.0, 0.0), axis=(0, 1), keepdims=True)
 
-    for load in loads[:3]:
+    for load in loads[:-1]:
         load.wait()
+    chosen = chosen_ref[...]
+    gain_row = jnp.concatenate([qg_ref[...], qg_ref[...]], axis=1)
+    q_gain = jnp.broadcast_to(gain_row, (2 * HD, 2 * HD)).T[:HD]
+    queries[:, HD:, :] = jnp.zeros((per_dev, HD, heads * BLOCK), BF16)
+    row_id = lax.broadcasted_iota(jnp.int32, chosen.shape, 0)
     kv = dot_nt(tok[...], wkv[...])
     lane = lax.broadcasted_iota(jnp.int32, (rows, 2 * HD), 1)
     is_key = lane < HD
@@ -121,47 +125,57 @@
 
     repeat(kv_n - 1, send)
 
-    loads[3].wait()
+    loads[-1].wait()
     query = jnp.dot(tok[...], wq[...], preferred_element_type=F32)
-    for h in range(heads):
-        qh = query[:, h * HD : (h + 1) * HD]
-        q_sq = jnp.mean(qh * qh, axis=-1, keepdims=True)
-        qh = (qh * lax.rsqrt(q_sq + EPSILON) * qg_ref[...] * HD**-0.5).astype(BF16)
-        qh = jnp.concatenate([qh, jnp.zeros((rows, HD), BF16)], axis=1)
+    for pair in range(heads // 2):
         for lb in range(per_dev):
-            queries[lb, h * BLOCK : (h + 1) * BLOCK] = qh[lb * BLOCK : (lb + 1) * BLOCK]
+            tile = query[lb * BLOCK : (lb + 1) * BLOCK, pair * 2 * HD : (pair + 1) * 2 * HD].T
+            for half in range(2):
+                qh = tile[half * HD : (half + 1) * HD]
+                q_sq = jnp.mean(qh * qh, axis=0, keepdims=True)
+                qh = qh * lax.rsqrt(q_sq + EPSILON) * q_gain * HD**-0.5
+                h = pair * 2 + half
+                queries[lb, :HD, h * BLOCK : (h + 1) * BLOCK] = qh.astype(BF16)
 
     lane_row = lax.broadcasted_iota(jnp.int32, (1, 2 * HD), 1)
     keep = jnp.where(lane_row < HD, 0.0, 1.0).astype(BF16)
     ones = jnp.where(lane_row < HD, 1.0, 0.0).astype(BF16)
 
-    def with_ones(block):
-        return block * keep + ones
-
-    q_pos = lax.rem(
-        lax.broadcasted_iota(jnp.int32, (heads * BLOCK, BLOCK), 0), BLOCK
-    )
-    causal = lax.broadcasted_iota(jnp.int32, (heads * BLOCK, BLOCK), 1) <= q_pos
+    def mix(weights, keyset):
+        return lax.dot_general(
+            keyset * keep + ones, weights, (((0,), (0,)), ((), ())), preferred_element_type=F32
+        )
+
+    span = heads * BLOCK
+    q_pos = lax.rem(lax.broadcasted_iota(jnp.int32, (BLOCK, span), 1), BLOCK)
+    causal = lax.broadcasted_iota(jnp.int32, (BLOCK, span), 0) <= q_pos
 
     def bias_of(cond):
-        return jnp.broadcast_to((1.0 - found(cond)) * NEGATIVE, (1, BLOCK))
+        return (1.0 - found(cond)) * NEGATIVE
+
+    def top(part):
+        return jnp.max(part, axis=0, keepdims=True)
+
+    def softmax_parts(parts, biases, peak):
+        for part, bias in zip(parts, biases):
+            level = top(part) if bias is None else top(part) + bias
+            peak = level if peak is None else jnp.maximum(peak, level)
+        weights = [
+            jnp.exp(part - (peak if bias is None else peak - bias)).astype(BF16)
+            for part, bias in zip(parts, biases)
+        ]
+        return peak, jnp.concatenate(weights, axis=0) if len(weights) > 1 else weights[0]
 
     state = []
     for lb in range(per_dev):
         mine_row = row_id == first + lb
-        scores = dot_nt(queries[lb], local[: (lb + 1) * BLOCK])
-        parts = [
-            scores[:, j * BLOCK : (j + 1) * BLOCK] + bias_of(mine_row & (chosen == first + j))
-            for j in range(lb)
-        ]
-        parts.append(jnp.where(causal, scores[:, lb * BLOCK :], NEGATIVE))
-        scores = jnp.concatenate(parts, axis=1) if lb else parts[0]
-        peak = jnp.max(scores, axis=-1, keepdims=True)
-        weights = jnp.exp(scores - peak).astype(BF16)
-        acc = jnp.dot(
-            weights, with_ones(local[: (lb + 1) * BLOCK]), preferred_element_type=F32
-        )
-        state.append((peak, acc))
+        keyset = local[: (lb + 1) * BLOCK]
+        scores = jnp.dot(keyset, queries[lb], preferred_element_type=F32)
+        parts = [scores[j * BLOCK : (j + 1) * BLOCK] for j in range(lb + 1)]
+        parts[lb] = jnp.where(causal, parts[lb], NEGATIVE)
+        biases = [bias_of(mine_row & (chosen == first + j)) for j in range(lb)] + [None]
+        peak, weights = softmax_parts(parts, biases, None)
+        state.append((peak, mix(weights, keyset)))
 
     def arrive(i):
         @pl.when(me - i - 1 >= 0)
@@ -177,13 +191,10 @@
             biases.append(
                 bias_of(mine_row & (chosen >= 0) & (chosen >= low) & (chosen < low + per_dev))
             )
-        scores = dot_nt(queries[lb], keyset) + jnp.concatenate(biases, axis=1)
-        peak_now = jnp.maximum(peak, jnp.max(scores, axis=-1, keepdims=True))
-        weights = jnp.exp(scores - peak_now).astype(BF16)
-        acc = acc * jnp.exp(peak - peak_now) + jnp.dot(
-            weights, with_ones(keyset), preferred_element_type=F32
-        )
-        return peak_now, acc
+        scores = jnp.dot(keyset, queries[lb], preferred_element_type=F32)
+        parts = [scores[g * BLOCK : (g + 1) * BLOCK] for g in range(group)]
+        peak_now, weights = softmax_parts(parts, biases, peak)
+        return peak_now, acc * jnp.exp(peak - peak_now) + mix(weights, keyset)
 
     def tp_copy(r, lb):
         return pltpu.make_async_remote_copy(
@@ -206,25 +217,24 @@
             peak, acc = lax.fori_loop(
                 0, groups, lambda n, c: merge(lb, n * group, *c), (peak, acc)
             )
-        totals = acc[:, :1]
-        mixed = acc[:, HD:]
-        m_sq = jnp.mean(mixed * mixed, axis=-1, keepdims=True)
+        totals = acc[:1]
+        mixed = acc[HD:]
+        m_sq = jnp.mean(mixed * mixed, axis=0, keepdims=True)
         normed = mixed * lax.rsqrt(m_sq + EPSILON * totals * totals)
-        for h in range(heads):
-            mine[lb, :, h * HD : (h + 1) * HD] = normed[h * BLOCK : (h + 1) * BLOCK].astype(BF16)
+        for pair in range(heads // 2):
+            both = [normed[:, h * BLOCK : (h + 1) * BLOCK] for h in (2 * pair, 2 * pair + 1)]
+            both = jnp.concatenate(both, axis=0).T
+            mine[lb, :, pair * 2 * HD : (pair + 1) * 2 * HD] = both.astype(BF16)
         for r in range(1, tp_n):
             tp_copy(r, lb).start()
 
-    loads[4].wait()
-    own_w = wo[pl.ds(pl.multiple_of(core * q_width, q_width), q_width), :]
     for lb in range(per_dev):
-        total = jnp.dot(mine[lb], own_w, preferred_element_type=F32)
+        block = slice(lb * BLOCK, (lb + 1) * BLOCK)
+        out_ref[block, pl.ds(pl.multiple_of(core * q_width, q_width), q_width)] = mine[lb]
         for r in range(1, tp_n):
             tp_copy(r, lb).wait_recv()
             src = lax.rem(core - r + tp_n, tp_n)
-            src_w = wo[pl.ds(pl.multiple_of(src * q_width, q_width), q_width), :]
-            total = total + jnp.dot(theirs[r - 1, lb], src_w, preferred_element_type=F32)
-        out_ref[lb * BLOCK : (lb + 1) * BLOCK, :] = total.astype(BF16)
+            out_ref[block, pl.ds(pl.multiple_of(src * q_width, q_width), q_width)] = theirs[r - 1, lb]
 
     def sent(i):
         @pl.when(me + i + 1 < kv_n)
@@ -244,34 +254,39 @@
     heads = q_width // HD
     group = next(g for g in (3, 2, 1) if (kv_n - 1) % g == 0)
     vmem = pl.BlockSpec(memory_space=pltpu.VMEM)
-    hbm = pl.BlockSpec(memory_space=pl.ANY)
-    return pl.pallas_call(
+    hbm = pl.BlockSpec(memory_space=pltpu.HBM)
+    attended = pl.pallas_call(
         functools.partial(kernel, kv_n, tp_n, group),
-        out_shape=jax.ShapeDtypeStruct((rows, w_out.shape[1]), BF16),
-        in_specs=[vmem] * 3 + [hbm] * 5,
+        out_shape=pltpu.VMEM((rows, tp_n * q_width), BF16),
+        in_specs=[hbm] * 7,
         out_specs=vmem,
         scratch_shapes=[
+            pltpu.VMEM(chosen.shape, jnp.int32),
+            pltpu.VMEM((1, HD), F32),
+            pltpu.VMEM((1, HD), F32),
             pltpu.VMEM((rows, depth), BF16),
             pltpu.VMEM((depth, q_width), BF16),
             pltpu.VMEM((2 * HD, depth), BF16),
-            pltpu.VMEM(w_out.shape, BF16),
             pltpu.VMEM((rows, 2 * HD), BF16),
             pltpu.VMEM((kv_n - 1, BLOCK, 2 * HD), BF16),
             pltpu.VMEM((kv_n - 1, BLOCK, 2 * HD), BF16),
-            pltpu.VMEM((per_dev, heads * BLOCK, 2 * HD), BF16),
+            pltpu.VMEM((per_dev, 2 * HD, heads * BLOCK), BF16),
             pltpu.VMEM((per_dev, BLOCK, q_width), BF16),
             pltpu.VMEM((tp_n - 1, per_dev, BLOCK, q_width), BF16),
-            pltpu.SemaphoreType.DMA((5,)),
+            pltpu.SemaphoreType.DMA((7,)),
             pltpu.SemaphoreType.DMA((kv_n - 1,)),
             pltpu.SemaphoreType.DMA((kv_n - 1,)),
             pltpu.SemaphoreType.DMA((tp_n - 1, per_dev)),
             pltpu.SemaphoreType.DMA((tp_n - 1, per_dev)),
         ],
-        compiler_params=pltpu.CompilerParams(collective_id=0, has_side_effects=True),
+        compiler_params=pltpu.CompilerParams(
+            collective_id=0, has_side_effects=True,
+        ),
     )(
         chosen, q_gain.reshape(1, HD), k_gain.reshape(1, HD),
-        tokens, w_query, w_key.T, w_value.T, w_out,
+        tokens, w_query, w_key.T, w_value.T,
     )
+    return jnp.dot(attended, w_out, preferred_element_type=F32).astype(BF16)
 
 
 def solution(mesh):

time: 14.3 us -> 11 us (0.77)
  the two profiles are of different devices: /device:TPU:9 before, /device:TPU:15 now
where the time goes in v2:
time: 11 us; the launch traced here: 10.8 us
  Pallas kernels  9.57 us (87%)
  matrix products  1.24 us (11%)
    pallas_call x1, Pallas kernels, on_device(): pl.pallas_call(functools.partial(kernel, kv_n, tp_n, group), out_shape=pl...  9.57 us
    dot_general x1, matrix products, on_device(): return jnp.dot(attended, w_out, preferred_element_type=F32).astype(BF16)  1.24 us

profile of v2, /device:TPU:15, one launch (start us, length us, event | category | flops | bytes accessed | tf_op | source)
XLA Modules:
  0.0 10.8 jit_solution(10631885393090510072)
XLA Ops:
  0.0 0.0 copy-start
  0.0 9.6 %shard_map.82 = bf16[256,512]{1,0:T(8,128)(2,1)S(1)} custom-call(s32[8,32]{1,0:T(8,128)} %chosen_hbm.1, f32[1,64]{1,0:T(1,128)} %bitcast.8, f32[1,64]{1,0:T(1,128)} %bitcast.9, bf16[256,2048]{1,0:T(8,128)(2,1)} %tok_hbm.1, bf16[2048,256]{1,0:T(8,128)(2,1)} %wq_hbm.1, bf16[64,2048]{1,0:T(8,128)(2,1)} %bitcast.6, bf16[64,2048]{1,0:T(8,128)(2,1)} %bitcast.7), custom_call_target="tpu_custom_call" | custom-call | tf_op jit(solution)/shard_map/pallas_call | solution.py:258
  9.6 0.0 copy-done
  9.6 1.2 %convolution_convert_fusion = bf16[256,1024]{1,0:T(8,128)(2,1)} fusion(bf16[256,512]{1,0:T(8,128)(2,1)S(1)} %shard_map.82, bf16[512,1024]{1,0:T(8,128)(2,1)S(1)} %copy-done), kind=kOutput, calls=%fused_computation | convolution fusion | flops 268697600 | bytes 1835008 | tf_op jit(solution)/shard_map/dot_general | solution.py:289
Async XLA Ops:
  0.0 9.6 %copy-start = (bf16[512,1024]{1,0:T(8,128)(2,1)S(1)}, bf16[512,1024]{1,0:T(8,128)(2,1)}, u32[]{:S(2)}) copy-start(bf16[512,1024]{1,0:T(8,128)(2,1)} %param.13) | copy-start | bytes 3145732

commit v3 on v2

v3 whole, which is shorter than its diff:
```python
import functools

import jax
import jax.numpy as jnp
from jax import lax
from jax.experimental import pallas as pl
from jax.experimental.pallas import tpu as pltpu
from jax.sharding import PartitionSpec as P

HD = 64
BLOCK = 128
NEGATIVE = -1e30
EPSILON = 1e-05
MESH = pl.DeviceIdType.MESH
F32 = jnp.float32
BF16 = jnp.bfloat16


def repeat(count, body):
    if count <= 8:
        for i in range(count):
            body(i)
    else:
        lax.fori_loop(0, count, lambda i, c: (body(i), c)[1], 0)


def dot_nt(a, b):
    return lax.dot_general(a, b, (((1,), (1,)), ((), ())), preferred_element_type=F32)


def kernel(
    kv_n, tp_n, group,
    chosen_hbm, qg_hbm, kg_hbm, tok_hbm, wq_hbm, wk_hbm, wv_hbm,
    out_ref,
    chosen_ref, qg_ref, kg_ref, tok, wq, wkv, local, stage, slots, queries, mine, theirs,
    load_sem, kv_send, kv_recv, tp_send, tp_recv,
):
    me = lax.axis_index("kv")
    core = lax.axis_index("tp")
    rows = tok.shape[0]
    per_dev = rows // BLOCK
    q_width = wq.shape[1]
    heads = q_width // HD
    first = me * per_dev

    loads = [
        pltpu.make_async_copy(chosen_hbm, chosen_ref, load_sem.at[0]),
        pltpu.make_async_copy(qg_hbm, qg_ref, load_sem.at[1]),
        pltpu.make_async_copy(kg_hbm, kg_ref, load_sem.at[2]),
        pltpu.make_async_copy(wk_hbm, wkv.at[pl.ds(0, HD)], load_sem.at[3]),
        pltpu.make_async_copy(wv_hbm, wkv.at[pl.ds(HD, HD)], load_sem.at[4]),
        pltpu.make_async_copy(tok_hbm, tok, load_sem.at[5]),
        pltpu.make_async_copy(wq_hbm, wq, load_sem.at[6]),
    ]

    barrier = pltpu.get_barrier_semaphore()

    def greet(i):
        @pl.when(me - i - 1 >= 0)
        def _():
            pl.semaphore_signal(
                barrier, inc=1, device_id={"kv": me - i - 1}, device_id_type=MESH
            )

    repeat(kv_n - 1, greet)
    for r in range(1, tp_n):
        pl.semaphore_signal(
            barrier, inc=1, device_id={"tp": lax.rem(core + r, tp_n)}, device_id_type=MESH
        )

    for load in loads[:-1]:
        load.start()

    def found(cond):
        return jnp.max(jnp.where(cond, 1.0, 0.0), axis=(0, 1), keepdims=True)

    for load in loads[:3]:
        load.wait()
    chosen = chosen_ref[...]
    row_id = lax.broadcasted_iota(jnp.int32, chosen.shape, 0)

    def column(gain):
        row = jnp.concatenate([gain, gain], axis=1)
        return jnp.broadcast_to(row, (2 * HD, 2 * HD)).T[:HD]

    q_gain = column(qg_ref[...])
    k_gain = column(kg_ref[...])
    short = kv_n <= 9

    def wants(i, j):
        dest = me + i + 1
        asked = (row_id >= dest * per_dev) & (row_id < (dest + 1) * per_dev)
        return found(asked & (chosen == first + j))

    def remote_bias(lb, i):
        low = (me - i - 1) * per_dev
        live = (chosen >= 0) & (chosen >= low) & (chosen < low + per_dev)
        return (1.0 - found((row_id == first + lb) & live)) * NEGATIVE

    wanted = [[wants(i, j) for j in range(1, per_dev)] for i in range(kv_n - 1)] if short else None
    remote_biases = (
        [[remote_bias(lb, i) for i in range(kv_n - 1)] for lb in range(per_dev)] if short else None
    )
    local_biases = [
        [(1.0 - found((row_id == first + lb) & (chosen == first + j))) * NEGATIVE for j in range(lb)]
        for lb in range(per_dev)
    ]

    for load in loads[3:-1]:
        load.wait()
    loads[-1].start()
    kv = dot_nt(wkv[...], tok[...])
    keys = kv[:HD]
    mean_sq = jnp.mean(keys * keys, axis=0, keepdims=True)
    keys = keys * lax.rsqrt(mean_sq + EPSILON)
    packed = []
    for j in range(per_dev):
        block = slice(j * BLOCK, (j + 1) * BLOCK)
        packed.append(jnp.concatenate([keys[:, block] * k_gain, kv[HD:, block]], axis=0))
        local[j] = packed[j].astype(BF16)

    def fill(i):
        dest = me + i + 1

        @pl.when(dest < kv_n)
        def _():
            sel = packed[0]
            for j in range(1, per_dev):
                hit = wanted[i][j - 1] if short else wants(i, j)
                hit = jnp.broadcast_to(hit, sel.shape)
                sel = jnp.where(hit > 0.5, packed[j], sel)
            stage[i] = sel.astype(BF16)

        @pl.when(me - i - 1 < 0)
        def _():
            slots[i] = jnp.zeros(slots.shape[1:], BF16)

    repeat(kv_n - 1, fill)

    pl.semaphore_wait(barrier, kv_n - 1 - me + tp_n - 1)

    def kv_copy(i, part):
        half = pl.ds(part * HD, HD)
        return pltpu.make_async_remote_copy(
            src_ref=stage.at[i, half],
            dst_ref=slots.at[i, half],
            send_sem=kv_send.at[part, i],
            recv_sem=kv_recv.at[part, i],
            device_id={"kv": lax.rem(me + i + 1, kv_n)},
            device_id_type=MESH,
        )

    def send(part, i):
        @pl.when(me + i + 1 < kv_n)
        def _():
            kv_copy(i, part).start()

    repeat(kv_n - 1, functools.partial(send, 0))
    repeat(kv_n - 1, functools.partial(send, 1))

    loads[-1].wait()
    query = jnp.dot(tok[...], wq[...], preferred_element_type=F32)
    for pair in range(heads // 2):
        for lb in range(per_dev):
            tile = query[lb * BLOCK : (lb + 1) * BLOCK, pair * 2 * HD : (pair + 1) * 2 * HD].T
            for half in range(2):
                qh = tile[half * HD : (half + 1) * HD]
                q_sq = jnp.mean(qh * qh, axis=0, keepdims=True)
                qh = qh * lax.rsqrt(q_sq + EPSILON) * q_gain * HD**-0.5
                h = pair * 2 + half
                queries[lb, :, h * BLOCK : (h + 1) * BLOCK] = qh.astype(BF16)

    def mix(weights, values):
        values = jnp.concatenate(values, axis=1) if len(values) > 1 else values[0]
        weights = jnp.concatenate(weights, axis=0) if len(weights) > 1 else weights[0]
        ones = jnp.ones((HD, values.shape[1]), BF16)
        return jnp.dot(
            jnp.concatenate([ones, values], axis=0), weights, preferred_element_type=F32
        )

    def scores_of(keyset, lb):
        return lax.dot_general(
            keyset, queries[lb], (((0,), (0,)), ((), ())), preferred_element_type=F32
        )

    span = heads * BLOCK
    q_pos = lax.rem(lax.broadcasted_iota(jnp.int32, (BLOCK, span), 1), BLOCK)
    causal = lax.broadcasted_iota(jnp.int32, (BLOCK, span), 0) <= q_pos

    def top(part):
        return jnp.max(part, axis=0, keepdims=True)

    def softmax_parts(parts, biases, peak):
        for part, bias in zip(parts, biases):
            level = top(part) if bias is None else top(part) + bias
            peak = level if peak is None else jnp.maximum(peak, level)
        weights = [
            jnp.exp(part - (peak if bias is None else peak - bias)).astype(BF16)
            for part, bias in zip(parts, biases)
        ]
        return peak, weights

    state = []
    for lb in range(per_dev):
        parts = [scores_of(local[j, :HD], lb) for j in range(lb + 1)]
        parts[lb] = jnp.where(causal, parts[lb], NEGATIVE)
        biases = local_biases[lb] + [None]
        peak, weights = softmax_parts(parts, biases, None)
        state.append((peak, mix(weights, [local[j, HD:] for j in range(lb + 1)])))

    def arrive(part, i):
        @pl.when(me - i - 1 >= 0)
        def _():
            kv_copy(i, part).wait_recv()

    def weigh(lb, base, peak):
        parts = [scores_of(slots[base + g, :HD], lb) for g in range(group)]
        biases = [
            remote_biases[lb][base + g] if short else remote_bias(lb, base + g)
            for g in range(group)
        ]
        return softmax_parts(parts, biases, peak)

    def add(base, before, peak, weights, acc):
        return acc * jnp.exp(before - peak) + mix(
            weights, [slots[base + g, HD:] for g in range(group)]
        )

    def merge(lb, n, carry):
        before, acc = carry
        peak, weights = weigh(lb, n * group, before)
        return peak, add(n * group, before, peak, weights, acc)

    def tp_copy(r, lb):
        return pltpu.make_async_remote_copy(
            src_ref=mine.at[lb],
            dst_ref=theirs.at[r - 1, lb],
            send_sem=tp_send.at[r - 1, lb],
            recv_sem=tp_recv.at[r - 1, lb],
            device_id={"tp": lax.rem(core + r, tp_n)},
            device_id_type=MESH,
        )

    groups = (kv_n - 1) // group
    single = short and groups == 1
    repeat(kv_n - 1, functools.partial(arrive, 0))
    if single:
        weighed = [weigh(lb, 0, state[lb][0]) for lb in range(per_dev)]
    repeat(kv_n - 1, functools.partial(arrive, 1))
    for lb in range(per_dev):
        before, acc = state[lb]
        if single:
            acc = add(0, before, *weighed[lb], acc)
        else:
            _, acc = lax.fori_loop(0, groups, functools.partial(merge, lb), state[lb])
        totals = acc[:1]
        mixed = acc[HD:]
        m_sq = jnp.mean(mixed * mixed, axis=0, keepdims=True)
        normed = mixed * lax.rsqrt(m_sq + EPSILON * totals * totals)
        for pair in range(heads // 2):
            both = [normed[:, h * BLOCK : (h + 1) * BLOCK] for h in (2 * pair, 2 * pair + 1)]
            both = jnp.concatenate(both, axis=0).T
            mine[lb, :, pair * 2 * HD : (pair + 1) * 2 * HD] = both.astype(BF16)
        for r in range(1, tp_n):
            tp_copy(r, lb).start()

    for lb in range(per_dev):
        block = slice(lb * BLOCK, (lb + 1) * BLOCK)
        out_ref[block, pl.ds(pl.multiple_of(core * q_width, q_width), q_width)] = mine[lb]
        for r in range(1, tp_n):
            tp_copy(r, lb).wait_recv()
            src = lax.rem(core - r + tp_n, tp_n)
            out_ref[block, pl.ds(pl.multiple_of(src * q_width, q_width), q_width)] = theirs[r - 1, lb]

    def sent(i):
        @pl.when(me + i + 1 < kv_n)
        def _():
            kv_copy(i, 0).wait_send()
            kv_copy(i, 1).wait_send()

    repeat(kv_n - 1, sent)
    for lb in range(per_dev):
        for r in range(1, tp_n):
            tp_copy(r, lb).wait_send()


def on_device(kv_n, tp_n, tokens, chosen, w_query, w_key, w_value, w_out, q_gain, k_gain):
    rows, depth = tokens.shape
    q_width = w_query.shape[1]
    per_dev = rows // BLOCK
    heads = q_width // HD
    group = next(g for g in (3, 2, 1) if (kv_n - 1) % g == 0)
    vmem = pl.BlockSpec(memory_space=pltpu.VMEM)
    hbm = pl.BlockSpec(memory_space=pltpu.HBM)
    attended = pl.pallas_call(
        functools.partial(kernel, kv_n, tp_n, group),
        out_shape=pltpu.VMEM((rows, tp_n * q_width), BF16),
        in_specs=[hbm] * 7,
        out_specs=vmem,
        scratch_shapes=[
            pltpu.VMEM(chosen.shape, jnp.int32),
            pltpu.VMEM((1, HD), F32),
            pltpu.VMEM((1, HD), F32),
            pltpu.VMEM((rows, depth), BF16),
            pltpu.VMEM((depth, q_width), BF16),
            pltpu.VMEM((2 * HD, depth), BF16),
            pltpu.VMEM((per_dev, 2 * HD, BLOCK), BF16),
            pltpu.VMEM((kv_n - 1, 2 * HD, BLOCK), BF16),
            pltpu.VMEM((kv_n - 1, 2 * HD, BLOCK), BF16),
            pltpu.VMEM((per_dev, HD, heads * BLOCK), BF16),
            pltpu.VMEM((per_dev, BLOCK, q_width), BF16),
            pltpu.VMEM((tp_n - 1, per_dev, BLOCK, q_width), BF16),
            pltpu.SemaphoreType.DMA((7,)),
            pltpu.SemaphoreType.DMA((2, kv_n - 1)),
            pltpu.SemaphoreType.DMA((2, kv_n - 1)),
            pltpu.SemaphoreType.DMA((tp_n - 1, per_dev)),
            pltpu.SemaphoreType.DMA((tp_n - 1, per_dev)),
        ],
        compiler_params=pltpu.CompilerParams(
            collective_id=0, has_side_effects=True,
        ),
    )(
        chosen, q_gain.reshape(1, HD), k_gain.reshape(1, HD),
        tokens, w_query, w_key.T, w_value.T,
    )
    return jnp.dot(attended, w_out, preferred_element_type=F32).astype(BF16)


def solution(mesh):
    placed = (
        P(("dp", "kv"), None),
        P("dp", None),
        P(None, "tp"),
        P(None, "tp"),
        P(None, "tp"),
        P(None, "tp"),
        P(),
        P(),
    )
    return jax.shard_map(
        functools.partial(on_device, mesh.shape["kv"], mesh.shape["tp"]),
        mesh=mesh, in_specs=placed, out_specs=P(("dp", "kv"), "tp"), check_vma=False,
    )
```

time: 11 us -> 10.3 us (0.936)
  the two profiles are of different devices: /device:TPU:15 before, /device:TPU:0 now
where the time goes in v3:
time: 10.3 us; the launch traced here: 10.1 us
  Pallas kernels  8.87 us (86%)
  matrix products  1.24 us (12%)
    pallas_call x1, Pallas kernels, on_device(): pl.pallas_call(functools.partial(kernel, kv_n, tp_n, group), out_shape=pl...  8.87 us
    dot_general x1, matrix products, on_device(): return jnp.dot(attended, w_out, preferred_element_type=F32).astype(BF16)  1.24 us

profile of v3, /device:TPU:0, one launch (start us, length us, event | category | flops | bytes accessed | tf_op | source)
XLA Modules:
  0.0 10.1 jit_solution(4116799628454469983)
XLA Ops:
  0.0 0.0 copy-start
  0.0 8.9 %shard_map.82 = bf16[256,512]{1,0:T(8,128)(2,1)S(1)} custom-call(s32[8,32]{1,0:T(8,128)} %chosen_hbm.1, f32[1,64]{1,0:T(1,128)} %bitcast.8, f32[1,64]{1,0:T(1,128)} %bitcast.9, bf16[256,2048]{1,0:T(8,128)(2,1)} %tok_hbm.1, bf16[2048,256]{1,0:T(8,128)(2,1)} %wq_hbm.1, bf16[64,2048]{1,0:T(8,128)(2,1)} %bitcast.6, bf16[64,2048]{1,0:T(8,128)(2,1)} %bitcast.7), custom_call_target="tpu_custom_call" | custom-call | tf_op jit(solution)/shard_map/pallas_call | solution.py:295
  8.9 0.0 copy-done
  8.9 1.2 %convolution_convert_fusion = bf16[256,1024]{1,0:T(8,128)(2,1)} fusion(bf16[256,512]{1,0:T(8,128)(2,1)S(1)} %shard_map.82, bf16[512,1024]{1,0:T(8,128)(2,1)S(1)} %copy-done), kind=kOutput, calls=%fused_computation | convolution fusion | flops 268697600 | bytes 1835008 | tf_op jit(solution)/shard_map/dot_general | solution.py:326
Async XLA Ops:
  0.0 8.9 %copy-start = (bf16[512,1024]{1,0:T(8,128)(2,1)S(1)}, bf16[512,1024]{1,0:T(8,128)(2,1)}, u32[]{:S(2)}) copy-start(bf16[512,1024]{1,0:T(8,128)(2,1)} %param.13) | copy-start | bytes 3145732
